TPU v7x, 32 devices: a whole 2x2x4 slice. The times are simulated.
32 devices in a mesh: grp: 2 (over y), sp: 4 (over z), tp: 4 (over x, core).
Axes of the slice: x: 2, y: 2, z: 4, core: 2. Of those that a mesh axis runs over, the one named last changes fastest.
Arguments:
- resid_in: bfloat16 [2048, 2048], P(('grp', 'sp', 'tp')), parts along dimension 0, may hold values from -6 to 6
- query_narrow: bfloat16 [2048, 8, 128], P(('grp', 'sp'), 'tp'), parts along dimension 0, may hold values from -512 to 512
- key_narrow: bfloat16 [2048, 4, 128], P(('grp', 'sp'), 'tp'), parts along dimension 0, may hold values from -512 to 512
- value_narrow: bfloat16 [2048, 4, 128], P(('grp', 'sp'), 'tp'), parts along dimension 0, may hold values from -6 to 6
- query_wide: bfloat16 [2048, 8, 256], P(('grp', 'sp'), 'tp'), parts along dimension 0, may hold values from -512 to 512
- key_wide: bfloat16 [2048, 4, 256], P(('grp', 'sp'), 'tp'), parts along dimension 0, may hold values from -512 to 512
- value_wide: bfloat16 [2048, 4, 128], P(('grp', 'sp'), 'tp'), parts along dimension 0, may hold values from -6 to 6
- lambda_narrow: float32 [8], P('tp'), may hold values from 0.3 to 0.8
- lambda_wide: float32 [8], P('tp'), may hold values from 0.3 to 0.8
- head_gain: float32 [128], replicated, may hold values from 0.1 to 1.9
- out_narrow: bfloat16 [1024, 2048], P('tp'), may hold values from -0.125 to 0.125
- out_wide: bfloat16 [1024, 2048], P('tp'), may hold values from -0.125 to 0.125
- norm_gain: bfloat16 [2048], replicated, may hold values from 0.099609375 to 1.8984375
- up_weight: bfloat16 [2048, 8192], P('sp', 'tp'), may hold values from -0.125 to 0.125
- down_weight: bfloat16 [8192, 2048], P('tp', 'sp'), may hold values from -0.0625 to 0.0625
Outputs:
- mixed_out: bfloat16 [2048, 2048], P(('grp', 'sp', 'tp')), parts along dimension 0
There are 2 independent parts, one for each index of `grp`. A program takes and returns all parts, laid end to end along the dimension named above; an argument that names none is the same for every part. Nothing has to cross between parts.
All inputs are finite; a program needn't handle non-finite values.
Results may differ from a plain program's by a relative error of at most 0.018.
Values may be sent and summed in bfloat16 or wider, within the bound.
A program may use at most 128 MiB of HBM per device.

v0:
```python
import math
import jax
import jax.numpy as jnp
from jax import lax
from jax.sharding import PartitionSpec as P

NORM_EPS = 1e-06
OUT_SCALE = 0.8


def empty_state(query, key_head_stack, value_width):
    row_count, head_count = (query.shape[0], query.shape[1])
    group_size = head_count // key_head_stack
    row_top = jnp.full((key_head_stack, group_size, 2, row_count), -jnp.inf, jnp.float32)
    row_total = jnp.zeros((key_head_stack, group_size, 2, row_count), jnp.float32)
    weighted_values = jnp.zeros(
        (key_head_stack, group_size, 2, row_count, value_width), jnp.float32
    )
    return (row_top, row_total, weighted_values)


def absorb(states, query, key_rows, values):
    row_count, head_count = (query.shape[0], query.shape[1])
    key_head_stack = key_rows.shape[1]
    half_width = key_rows.shape[2] // 2
    group_size = head_count // key_head_stack
    value_width = values.shape[2]
    amount = key_rows.shape[0]
    block_rows = math.gcd(amount, 512)
    rotation_count = amount // block_rows
    grouped = query.reshape(row_count, key_head_stack, group_size, 2, half_width)
    key_block_list = key_rows.reshape(rotation_count, block_rows, key_head_stack, 2, half_width)
    value_blocks = values.reshape(rotation_count, block_rows, key_head_stack, value_width)

    def visit(running, kv_pair):
        row_top, row_total, weighted_values = running
        key_blk, value_blk = kv_pair
        scores = jnp.einsum(
            "tkgcd,skcd->kgcts", grouped, key_blk, preferred_element_type=jnp.float32
        ) * half_width ** (-0.5)
        new_top = jnp.maximum(row_top, jnp.max(scores, axis=-1))
        rescale = jnp.exp(row_top - new_top)
        powers = jnp.exp(scores - new_top[..., None])
        row_total = row_total * rescale + jnp.sum(powers, axis=-1)
        weighted_values = weighted_values * rescale[..., None] + jnp.einsum(
            "iodph,hie->iodpe",
            powers.astype(jnp.bfloat16),
            value_blk,
            preferred_element_type=jnp.float32,
        )
        return ((new_top, row_total, weighted_values), None)

    outcome, _ = lax.scan(visit, states, (key_block_list, value_blocks))
    return outcome


def finish(states, lambdas, gain_vec):
    row_top, row_total, weighted_values = states
    key_head_stack, group_size, row_count = (row_top.shape[0], row_top.shape[1], row_top.shape[3])
    value_width = weighted_values.shape[4]
    first_map = weighted_values[:, :, 0] / row_total[:, :, 0, :, None]
    second_map = weighted_values[:, :, 1] / row_total[:, :, 1, :, None]
    mixed = first_map - lambdas.reshape(key_head_stack, group_size)[:, :, None, None] * second_map
    normed = (
        mixed
        * lax.rsqrt(jnp.mean(mixed * mixed, axis=-1, keepdims=True) + NORM_EPS)
        * gain_vec
        * OUT_SCALE
    )
    normed = normed.astype(jnp.bfloat16).transpose(2, 0, 1, 3)
    return normed.reshape(row_count, key_head_stack * group_size * value_width)


def attend(
    query_narrow,
    key_narrow,
    value_narrow,
    query_wide,
    key_wide,
    value_wide,
    lambda_narrow,
    lambda_wide,
    head_gain,
):
    initial = (
        empty_state(query_narrow, key_narrow.shape[1], value_narrow.shape[2]),
        empty_state(query_wide, key_wide.shape[1], value_wide.shape[2]),
    )
    narrow_keys = lax.all_gather(key_narrow, "sp", axis=0, tiled=True)
    narrow_values = lax.all_gather(value_narrow, "sp", axis=0, tiled=True)
    wide_keys = lax.all_gather(key_wide, "sp", axis=0, tiled=True)
    wide_values = lax.all_gather(value_wide, "sp", axis=0, tiled=True)
    narrow_state = absorb(initial[0], query_narrow, narrow_keys, narrow_values)
    wide_state = absorb(initial[1], query_wide, wide_keys, wide_values)
    return (
        finish(narrow_state, lambda_narrow, head_gain),
        finish(wide_state, lambda_wide, head_gain),
    )


def shards(
    resid_in,
    query_narrow,
    key_narrow,
    value_narrow,
    query_wide,
    key_wide,
    value_wide,
    lambda_narrow,
    lambda_wide,
    head_gain,
    out_narrow,
    out_wide,
    norm_gain,
    up_weight,
    down_weight,
):
    att_narrow, att_wide = attend(
        query_narrow,
        key_narrow,
        value_narrow,
        query_wide,
        key_wide,
        value_wide,
        lambda_narrow,
        lambda_wide,
        head_gain,
    )
    projected = lax.psum_scatter(
        (
            jnp.dot(att_narrow, out_narrow, preferred_element_type=jnp.float32)
            + jnp.dot(att_wide, out_wide, preferred_element_type=jnp.float32)
        ).astype(jnp.bfloat16),
        "tp",
        scatter_dimension=0,
        tiled=True,
    ).astype(jnp.float32)
    middle = (resid_in.astype(jnp.float32) + projected).astype(jnp.bfloat16)
    middle_f32 = middle.astype(jnp.float32)
    normed = middle_f32 * lax.rsqrt(
        jnp.mean(middle_f32 * middle_f32, axis=-1, keepdims=True) + NORM_EPS
    )
    normed = (normed * norm_gain.astype(jnp.float32)).astype(jnp.bfloat16)
    whole_rows = lax.all_gather(normed, "tp", axis=0, tiled=True)
    up_collected = lax.all_gather(up_weight, "sp", axis=0, tiled=True)
    lifted = jnp.dot(whole_rows, up_collected, preferred_element_type=jnp.float32)
    activated = jnp.square(jax.nn.relu(lifted)).astype(jnp.bfloat16)
    partials = jnp.dot(
        activated,
        lax.all_gather(down_weight, "sp", axis=1, tiled=True),
        preferred_element_type=jnp.float32,
    )
    mixer_out = lax.psum_scatter(
        partials.astype(jnp.bfloat16), "tp", scatter_dimension=0, tiled=True
    ).astype(jnp.float32)
    return (middle_f32 + mixer_out).astype(jnp.bfloat16)


def solution(mesh):
    placed = (
        P(("grp", "sp", "tp"), None),
        P(("grp", "sp"), "tp", None),
        P(("grp", "sp"), "tp", None),
        P(("grp", "sp"), "tp", None),
        P(("grp", "sp"), "tp", None),
        P(("grp", "sp"), "tp", None),
        P(("grp", "sp"), "tp", None),
        P("tp"),
        P("tp"),
        P(),
        P("tp", None),
        P("tp", None),
        P(),
        P("sp", "tp"),
        P("tp", "sp"),
    )
    return jax.shard_map(
        shards, mesh=mesh, in_specs=placed, out_specs=P(("grp", "sp", "tp"), None), check_vma=False
    )
```

profile of v0, /device:TPU:0, one launch (start us, length us, event | category | flops | bytes accessed | tf_op | source)
XLA Modules:
  0.0 480.9 jit_solution(12649065433829812458)
XLA Ops:
  6.6 17.7 %all_gather.23 = bf16[1024,1,256]{2,0,1:T(8,128)(2,1)S(1)} all-gather(bf16[256,1,256]{2,0,1:T(8,128)(2,1)} %param.24), channel_id=1, replica_groups=mesh['grp'=2,'sp'=4,'tp'=4] {'sp'}, dimensions={0}, use_global_device_ids=true | all-gather | bytes 655360 | tf_op jit(solution)/shard_map/all_gather | solution.py:91
  24.4 1.1 copy.33
  25.5 0.2 copy.35
  25.7 15.3 %all_gather.24 = bf16[1024,1,128]{2,0,1:T(8,128)(2,1)} all-gather(bf16[256,1,128]{2,0,1:T(8,128)(2,1)S(1)} %copy-done.9), channel_id=1, replica_groups=mesh['grp'=2,'sp'=4,'tp'=4] {'sp'}, dimensions={0}, use_global_device_ids=true | all-gather | bytes 327680 | tf_op jit(solution)/shard_map/all_gather | solution.py:92
  41.1 8.2 %while.31 = (s32[]{:T(128)}, f32[1,2,2,256]{3,1,2,0:T(2,128)S(1)}, f32[1,2,2,256]{3,1,2,0:T(2,128)S(1)}, f32[1,2,2,256,128]{4,3,2,1,0:T(8,128)}, bf16[2,512,1,2,...) while((s32[]{:T(128)}, f32[1,2,2,256]{3,1,2,0:T(2,128)S(1)}, ...), condition=%wide.region_8.9_spmd.clone, body=%wide.region_5.0_spmd.clone.sunk | while | flops 271980544 | bytes 13832389 | solution.py:53
  41.1 0.2 constant_dynamic-slice_fusion.2
  41.3 0.6 copy-done.1
  41.9 0.4 bitcast_reduce_fusion.5
  42.4 0.4 fusion.71
  42.8 0.5 copy-done.7
  43.3 1.3 fusion.72
  44.7 0.2 constant_dynamic-slice_fusion.2
  44.9 0.6 copy-done.1
  45.5 0.4 bitcast_reduce_fusion.5
  46.0 0.4 fusion.71
  46.4 0.5 copy-done.7
  46.9 2.3 fusion.72
  49.3 0.6 slice_bitcast_fusion.5
  49.9 14.2 %all_gather.21 = bf16[1024,1,128]{2,0,1:T(8,128)(2,1)S(1)} all-gather(bf16[256,1,128]{2,0,1:T(8,128)(2,1)S(1)} %copy-done.10), channel_id=1, replica_groups=mesh['grp'=2,'sp'=4,'tp'=4] {'sp'}, dimensions={0}, use_global_device_ids=true | all-gather | bytes 327680 | tf_op jit(solution)/shard_map/all_gather | solution.py:89
  64.1 0.2 reshape.272
  64.3 0.4 copy.29
  64.7 15.6 %all_gather.22 = bf16[1024,1,128]{2,0,1:T(8,128)(2,1)} all-gather(bf16[256,1,128]{2,0,1:T(8,128)(2,1)} %param.22), channel_id=1, replica_groups=mesh['grp'=2,'sp'=4,'tp'=4] {'sp'}, dimensions={0}, use_global_device_ids=true | all-gather | bytes 327680 | tf_op jit(solution)/shard_map/all_gather | solution.py:90
  80.5 6.6 %while.30 = (s32[]{:T(128)}, f32[1,2,2,256]{3,1,2,0:T(2,128)S(1)}, f32[1,2,2,256]{3,1,2,0:T(2,128)S(1)}, f32[1,2,2,256,128]{4,3,2,1,0:T(8,128)}, bf16[2,512,1,2,...) while((s32[]{:T(128)}, f32[1,2,2,256]{3,1,2,0:T(2,128)S(1)}, ...), condition=%wide.region_3.4_spmd.clone, body=%wide.region_0.3_spmd.clone.sunk | while | flops 204871680 | bytes 8851597 | solution.py:53
  80.5 0.5 bitcast_reduce_fusion.4
  81.1 0.4 fusion.66
  81.5 0.5 copy-done.6
  82.0 1.3 fusion.67
  83.3 0.5 bitcast_reduce_fusion.4
  83.9 0.4 fusion.66
  84.3 0.5 copy-done.6
  84.8 2.3 fusion.67
  87.2 1.2 copy.36
  88.5 1.2 copy.31
  89.7 0.2 multiply_reduce_fusion
  90.1 0.5 fusion.45
  90.6 0.6 copy-done.5
  91.2 1.4 fusion.29
  92.7 25.0 %reduce-scatter.3.cloned.1.call-done = bf16[64,2048]{1,0:T(8,128)(2,1)} async-done(((bf16[256,2048]{1,0:T(8,128)(2,1)}), bf16[64,2048]{1,0:T(8,128)(2,1)}) %reduce-scatter.3.cloned.1.call-update) | async-done | bytes 262160 | tf_op jit(solution)/shard_map/reduce_scatter | solution.py:129
  117.7 1.1 fusion.30
  118.8 1.8 fusion.32
  120.7 0.7 all-gather.6.cloned.1.call-update
  121.4 0.5 all-gather.8.cloned.1.call-update
  122.0 15.5 %all-gather.4.cloned.1.call-done = bf16[256,2048]{1,0:T(8,128)(2,1)} async-done(((bf16[64,2048]{1,0:T(8,128)(2,1)}), bf16[256,2048]{1,0:T(8,128)(2,1)}) %all-gather.4.cloned.1.call-update) | async-done | bytes 1048592 | tf_op jit(solution)/shard_map/all_gather | solution.py:144
  137.4 151.2 %all-gather.6.cloned.1.call-done = bf16[2048,2048]{1,0:T(8,128)(2,1)} async-done(((bf16[512,2048]{1,0:T(8,128)(2,1)}), bf16[2048,2048]{1,0:T(8,128)(2,1)}) %all-gather.6.cloned.1.call-update) | async-done | bytes 8388624 | tf_op jit(solution)/shard_map/all_gather | solution.py:145
  288.7 149.3 %all-gather.8.cloned.1.call-done = bf16[2048,2048]{1,0:T(8,128)(2,1)} async-done(((bf16[2048,512]{1,0:T(8,128)(2,1)}), bf16[2048,2048]{1,0:T(8,128)(2,1)}) %all-gather.8.cloned.1.call-update) | async-done | bytes 8388624 | tf_op jit(solution)/shard_map/all_gather | solution.py:150
  437.9 11.5 %convolution_convert_fusion = bf16[256,2048]{1,0:T(8,128)(2,1)} fusion(bf16[2048,2048]{1,0:T(8,128)(2,1)} %all-gather.8.cloned.1.call-done, bf16[256,2048]{1,0:T(8,128)(2,1)} %all-gather.4.cloned.1.call-done, bf16[2048,2048]{1,0:T(8,128)(2,1)} %all-gather.6.cloned.1.call-done), kind=kOutput, calls=%fused_computation.52 | convolution fusion | flops 4297064448 | bytes 18874368 | tf_op jit(solution)/shard_map/dot_general | solution.py:148
  449.5 23.1 %reduce-scatter.5.cloned.1.call-done = bf16[64,2048]{1,0:T(8,128)(2,1)} async-done(((bf16[256,2048]{1,0:T(8,128)(2,1)}), bf16[64,2048]{1,0:T(8,128)(2,1)}) %reduce-scatter.5.cloned.1.call-update) | async-done | bytes 262160 | tf_op jit(solution)/shard_map/reduce_scatter | solution.py:153
  472.6 1.7 fusion.33
  (72 shorter events, 0.8 us)
Async XLA Ops:
  6.5 83.6 %copy-start = (bf16[256,2048]{1,0:T(8,128)(2,1)S(1)}, bf16[256,2048]{1,0:T(8,128)(2,1)}, u32[]{:S(2)}) copy-start(bf16[256,2048]{1,0:T(8,128)(2,1)} %param.29) | copy-start | bytes 3145732
  6.5 19.2 %copy-start.9 = (bf16[256,1,128]{2,0,1:T(8,128)(2,1)S(1)}, bf16[256,1,128]{2,0,1:T(8,128)(2,1)}, u32[]{:S(2)}) copy-start(bf16[256,1,128]{2,0,1:T(8,128)(2,1)} %param.25) | copy-start | bytes 196612
  6.5 111.1 %reduce-scatter.3.cloned.1.call-start = ((), (), s32[]{:S(2)}) async-start(), calls=%async_computation.2 | async-start | bytes 1310720 | tf_op jit(solution)/shard_map/reduce_scatter | solution.py:129
  41.1 8.8 %copy-start.10 = (bf16[256,1,128]{2,0,1:T(8,128)(2,1)S(1)}, bf16[256,1,128]{2,0,1:T(8,128)(2,1)}, u32[]{:S(2)}) copy-start(bf16[256,1,128]{2,0,1:T(8,128)(2,1)} %param.21) | copy-start | bytes 196612
  41.1 0.8 copy-start.1
  42.4 1.0 copy-start.7
  42.8 1.8 copy-start.2
  44.7 0.8 copy-start.1
  45.9 1.0 copy-start.7
  46.4 2.9 copy-start.2
  49.3 31.1 %copy-start.8 = (bf16[256,2,128]{2,1,0:T(2,128)(2,1)S(1)}, bf16[256,2,128]{2,1,0:T(2,128)(2,1)}, u32[]{:S(2)}) copy-start(bf16[256,2,128]{2,1,0:T(2,128)(2,1)} %param.20) | copy-start | bytes 393220
  81.0 1.0 copy-start.6
  83.8 1.0 copy-start.6
  87.2 2.6 copy-start.11
  87.2 2.6 copy-start.13
  87.2 2.6 copy-start.14
  87.2 2.8 copy-start.15
  89.9 1.2 copy-start.5
  91.2 1.5 copy-start.12
  91.2 26.5 %copy-start.3 = (bf16[64,2048]{1,0:T(8,128)(2,1)S(1)}, bf16[64,2048]{1,0:T(8,128)(2,1)}, u32[]{:S(2)}) copy-start(bf16[64,2048]{1,0:T(8,128)(2,1)} %param.19) | copy-start | bytes 786436
  92.6 44.8 %all-gather.4.cloned.1.call-start = ((), (), s32[]{:S(2)}) async-start(), calls=%async_computation.3 | async-start | bytes 1310720 | tf_op jit(solution)/shard_map/all_gather | solution.py:144
  120.6 168.1 %all-gather.6.cloned.1.call-start = ((), (), s32[]{:S(2)}) async-start(), calls=%async_computation.4 | async-start | bytes 10485760 | tf_op jit(solution)/shard_map/all_gather | solution.py:145
  121.3 316.6 %all-gather.8.cloned.1.call-start = ((), (), s32[]{:S(2)}) async-start(), calls=%async_computation.5 | async-start | bytes 10485760 | tf_op jit(solution)/shard_map/all_gather | solution.py:150
  121.9 350.7 %copy-start.4 = (bf16[64,2048]{1,0:T(8,128)(2,1)S(1)}, bf16[64,2048]{1,0:T(8,128)(2,1)}, u32[]{:S(2)}) copy-start(bf16[64,2048]{1,0:T(8,128)(2,1)} %reduce-scatter.3.cloned.1.call-done) | copy-start | bytes 786436
  121.9 350.7 %reduce-scatter.5.cloned.1.call-start = ((), (), s32[]{:S(2)}) async-start(), calls=%async_computation.6 | async-start | bytes 1310720 | tf_op jit(solution)/shard_map/reduce_scatter | solution.py:153
Sparse Core Ops, SparseCore 0:
  92.7 24.8 reduce-scatter.2
  120.7 16.6 all-gather.3
  139.0 149.6 all-gather.5
  290.1 147.7 all-gather.7
  449.6 22.9 reduce-scatter.4
where the time goes:
time: 481 us
  waiting for transfers between devices  365 us (76%)
  blocking collectives  62.9 us (13%)
  matrix products  22.6 us (5%)
  between operations  13.4 us (3%)
  local copies, waits for them, and re-layouts  9.51 us (2%)
  other arithmetic  6.74 us (1%)
    all_gather x1, waiting for transfers between devices, shards(): up_collected = lax.all_gather(up_weight, 'sp', axis=0, tiled=True)  151 us
    all_gather x1, waiting for transfers between devices, shards(): lax.all_gather(down_weight, 'sp', axis=1, tiled=True)  149 us
    reduce_scatter x1, waiting for transfers between devices, shards(): lax.psum_scatter((jnp.dot(att_narrow, out_narrow, preferred_element_type=...  25 us
    reduce_scatter x1, waiting for transfers between devices, shards(): lax.psum_scatter(partials.astype(jnp.bfloat16), 'tp', scatter_dimension=0...  23.1 us
    all_gather x1, blocking collectives, attend(): wide_keys = lax.all_gather(key_wide, 'sp', axis=0, tiled=True)  17.7 us
    all_gather x1, blocking collectives, attend(): narrow_values = lax.all_gather(value_narrow, 'sp', axis=0, tiled=True)  15.6 us
    all_gather x1, waiting for transfers between devices, shards(): whole_rows = lax.all_gather(normed, 'tp', axis=0, tiled=True)  15.5 us
    all_gather x1, blocking collectives, attend(): wide_values = lax.all_gather(value_wide, 'sp', axis=0, tiled=True)  15.3 us
  transfers between devices with their start and end apart: 5, of which 5 were waited for; matrix products, arithmetic and copies ran while one was open for 0% of the time, Pallas kernels for 0%

commit v1 on v0

--- a/solution.py
+++ b/solution.py
@@ -3,6 +3,7 @@
 import jax.numpy as jnp
 from jax import lax
 from jax.sharding import PartitionSpec as P
+from jax.lax import all_gather
 
 NORM_EPS = 1e-06
 OUT_SCALE = 0.8
@@ -115,6 +116,11 @@
     up_weight,
     down_weight,
 ):
+
+    def view_lanes(state):
+        res = jnp.concatenate(all_gather(state, "sp"), axis=1)
+        return res
+
     att_narrow, att_wide = attend(
         query_narrow,
         key_narrow,
@@ -145,11 +151,7 @@
     up_collected = lax.all_gather(up_weight, "sp", axis=0, tiled=True)
     lifted = jnp.dot(whole_rows, up_collected, preferred_element_type=jnp.float32)
     activated = jnp.square(jax.nn.relu(lifted)).astype(jnp.bfloat16)
-    partials = jnp.dot(
-        activated,
-        lax.all_gather(down_weight, "sp", axis=1, tiled=True),
-        preferred_element_type=jnp.float32,
-    )
+    partials = jnp.dot(activated, view_lanes(down_weight), preferred_element_type=jnp.float32)
     mixer_out = lax.psum_scatter(
         partials.astype(jnp.bfloat16), "tp", scatter_dimension=0, tiled=True
     ).astype(jnp.float32)

time: 481 us -> 456 us (0.948)
  waiting for transfers between devices: 365 us -> 327 us
  local copies, waits for them, and re-layouts: 9.51 us -> 24.7 us
    all_gather x1, waiting for transfers between devices: 149 us -> 123 us  [view_lanes(): res = jnp.concatenate(all_gather(state, 'sp'), axis=1)]
    reshape x0 -> x1, local copies, waits for them, and re-layouts: none -> 11.5 us  [view_lanes(): res = jnp.concatenate(all_gather(state, 'sp'), axis=1)]
    all_gather x1, waiting for transfers between devices: 15.5 us -> 4.74 us  [shards(): whole_rows = lax.all_gather(normed, 'tp', axis=0, tiled=True)]
  transfers between devices with their start and end apart: 5 -> 5, of which waited for: 5 -> 5; matrix products, arithmetic and copies ran while one was open for 0% -> 3% of each run, Pallas kernels for 0% -> 0%
where the time goes in v1:
time: 456 us; the launch traced here: 455 us
  waiting for transfers between devices  327 us (72%)
  blocking collectives  62.9 us (14%)
  local copies, waits for them, and re-layouts  24.7 us (5%)
  matrix products  18 us (4%)
  between operations  15.3 us (3%)
  other arithmetic  6.74 us (1%)
    all_gather x1, waiting for transfers between devices, shards(): up_collected = lax.all_gather(up_weight, 'sp', axis=0, tiled=True)  151 us
    all_gather x1, waiting for transfers between devices, view_lanes(): res = jnp.concatenate(all_gather(state, 'sp'), axis=1)  123 us
    reduce_scatter x1, waiting for transfers between devices, shards(): lax.psum_scatter((jnp.dot(att_narrow, out_narrow, preferred_element_type=...  24.4 us
    reduce_scatter x1, waiting for transfers between devices, shards(): lax.psum_scatter(partials.astype(jnp.bfloat16), 'tp', scatter_dimension=0...  23.1 us
    all_gather x1, blocking collectives, attend(): wide_keys = lax.all_gather(key_wide, 'sp', axis=0, tiled=True)  17.7 us
    all_gather x1, blocking collectives, attend(): narrow_values = lax.all_gather(value_narrow, 'sp', axis=0, tiled=True)  15.6 us
    all_gather x1, blocking collectives, attend(): wide_values = lax.all_gather(value_wide, 'sp', axis=0, tiled=True)  15.3 us
    all_gather x1, blocking collectives, attend(): narrow_keys = lax.all_gather(key_narrow, 'sp', axis=0, tiled=True)  14.2 us
  transfers between devices with their start and end apart: 5, of which 5 were waited for; matrix products, arithmetic and copies ran while one was open for 3% of the time, Pallas kernels for 0%

profile of v1, /device:TPU:0, one launch (start us, length us, event | category | flops | bytes accessed | tf_op | source)
XLA Modules:
  0.0 455.4 jit_solution(3938996647065552609)
XLA Ops:
  7.4 17.7 %all_gather.26 = bf16[1024,1,256]{2,0,1:T(8,128)(2,1)S(1)} all-gather(bf16[256,1,256]{2,0,1:T(8,128)(2,1)} %param.24), channel_id=1, replica_groups=mesh['grp'=2,'sp'=4,'tp'=4] {'sp'}, dimensions={0}, use_global_device_ids=true | all-gather | bytes 655360 | tf_op jit(solution)/shard_map/all_gather | solution.py:92
  25.3 1.1 copy.48
  26.6 15.3 %all_gather.27 = bf16[1024,1,128]{2,0,1:T(8,128)(2,1)} all-gather(bf16[256,1,128]{2,0,1:T(8,128)(2,1)S(1)} %copy-done.13), channel_id=1, replica_groups=mesh['grp'=2,'sp'=4,'tp'=4] {'sp'}, dimensions={0}, use_global_device_ids=true | all-gather | bytes 327680 | tf_op jit(solution)/shard_map/all_gather | solution.py:93
  41.9 7.7 %while.31 = (s32[]{:T(128)}, f32[1,2,2,256]{3,1,2,0:T(2,128)S(1)}, f32[1,2,2,256]{3,1,2,0:T(2,128)S(1)}, f32[1,2,2,256,128]{4,3,2,1,0:T(8,128)}, bf16[2,512,1,2,...) while((s32[]{:T(128)}, f32[1,2,2,256]{3,1,2,0:T(2,128)S(1)}, ...), condition=%wide.region_8.9_spmd.clone, body=%wide.region_5.0_spmd.clone.sunk | while | flops 271980544 | bytes 18026748 | solution.py:54
  42.1 0.6 copy-done.1
  42.7 0.4 bitcast_reduce_fusion.5
  43.2 0.4 fusion.71
  43.7 0.6 copy-done.8
  44.3 0.6 fusion.72
  44.9 0.8 copy-done.9
  46.0 0.6 copy-done.1
  46.6 0.4 bitcast_reduce_fusion.5
  47.1 0.4 fusion.71
  47.5 0.6 copy-done.8
  48.1 0.6 fusion.72
  48.8 0.8 copy-done.9
  49.6 0.6 slice_bitcast_fusion.5
  50.2 14.2 %all_gather.24 = bf16[1024,1,128]{2,0,1:T(8,128)(2,1)S(1)} all-gather(bf16[256,1,128]{2,0,1:T(8,128)(2,1)S(1)} %copy-done.14), channel_id=1, replica_groups=mesh['grp'=2,'sp'=4,'tp'=4] {'sp'}, dimensions={0}, use_global_device_ids=true | all-gather | bytes 327680 | tf_op jit(solution)/shard_map/all_gather | solution.py:90
  64.6 0.4 copy.44
  65.0 15.6 %all_gather.25 = bf16[1024,1,128]{2,0,1:T(8,128)(2,1)} all-gather(bf16[256,1,128]{2,0,1:T(8,128)(2,1)} %param.22), channel_id=1, replica_groups=mesh['grp'=2,'sp'=4,'tp'=4] {'sp'}, dimensions={0}, use_global_device_ids=true | all-gather | bytes 327680 | tf_op jit(solution)/shard_map/all_gather | solution.py:91
  80.8 6.2 %while.30 = (s32[]{:T(128)}, f32[1,2,2,256]{3,1,2,0:T(2,128)S(1)}, f32[1,2,2,256]{3,1,2,0:T(2,128)S(1)}, f32[1,2,2,256,128]{4,3,2,1,0:T(8,128)}, bf16[2,512,1,2,...) while((s32[]{:T(128)}, f32[1,2,2,256]{3,1,2,0:T(2,128)S(1)}, ...), condition=%wide.region_3.4_spmd.clone, body=%wide.region_0.3_spmd.clone.sunk | while | flops 204871680 | bytes 13045957 | solution.py:54
  80.8 0.5 bitcast_reduce_fusion.4
  81.4 0.4 fusion.66
  81.8 0.6 copy-done.6
  82.5 0.6 fusion.67
  83.1 0.8 copy-done.7
  83.9 0.5 bitcast_reduce_fusion.4
  84.5 0.4 fusion.66
  84.9 0.6 copy-done.6
  85.5 0.6 fusion.67
  86.2 0.8 copy-done.7
  87.0 1.2 copy.51
  88.3 1.2 copy.46
  89.9 0.5 fusion.45
  90.4 0.6 copy-done.5
  91.0 1.5 fusion.29
  92.5 0.5 all-gather.9.cloned.1.call-update
  93.1 24.4 %reduce-scatter.3.cloned.1.call-done = bf16[64,2048]{1,0:T(8,128)(2,1)} async-done(((bf16[256,2048]{1,0:T(8,128)(2,1)}), bf16[64,2048]{1,0:T(8,128)(2,1)}) %reduce-scatter.3.cloned.1.call-update) | async-done | bytes 262160 | tf_op jit(solution)/shard_map/reduce_scatter | solution.py:135
  117.5 1.1 fusion.30
  118.7 1.8 fusion.32
  120.5 0.5 all-gather.7.cloned.1.call-update
  121.1 123.0 %all-gather.9.cloned.1.call-done = bf16[8192,512]{1,0:T(8,128)(2,1)} async-done(((bf16[2048,512]{1,0:T(8,128)(2,1)}), bf16[8192,512]{1,0:T(8,128)(2,1)}) %all-gather.9.cloned.1.call-update) | async-done | bytes 8388624 | tf_op jit(solution)/shard_map/all_gather | solution.py:121
  244.1 11.5 %copy.53 = bf16[2048,4,512]{0,2,1:T(8,128)(2,1)} copy(bf16[2048,4,512]{2,0,1:T(8,128)(2,1)} %bitcast.201) | data formatting | bytes 16777216 | tf_op jit(solution)/shard_map/reshape | solution.py:121
  255.6 4.7 %all-gather.5.cloned.1.call-done = bf16[256,2048]{1,0:T(8,128)(2,1)} async-done(((bf16[64,2048]{1,0:T(8,128)(2,1)}), bf16[256,2048]{1,0:T(8,128)(2,1)}) %all-gather.5.cloned.1.call-update) | async-done | bytes 1048592 | tf_op jit(solution)/shard_map/all_gather | solution.py:150
  260.3 150.9 %all-gather.7.cloned.1.call-done = bf16[2048,2048]{1,0:T(8,128)(2,1)} async-done(((bf16[512,2048]{1,0:T(8,128)(2,1)}), bf16[2048,2048]{1,0:T(8,128)(2,1)}) %all-gather.7.cloned.1.call-update) | async-done | bytes 8388624 | tf_op jit(solution)/shard_map/all_gather | solution.py:151
  411.3 11.7 %convolution_convert_fusion = bf16[256,2048]{1,0:T(8,128)(2,1)} fusion(bf16[2048,2048]{0,1:T(8,128)(2,1)} %bitcast.202, bf16[256,2048]{1,0:T(8,128)(2,1)} %all-gather.5.cloned.1.call-done, bf16[2048,2048]{1,0:T(8,128)(2,1)} %all-gather.7.cloned.1.call-done), kind=kOutput, calls=%fused_computation.52 | convolution fusion | flops 4297064448 | bytes 18874368 | tf_op jit(solution)/shard_map/dot_general | solution.py:154
  423.0 23.1 %reduce-scatter.5.cloned.1.call-done = bf16[64,2048]{1,0:T(8,128)(2,1)} async-done(((bf16[256,2048]{1,0:T(8,128)(2,1)}), bf16[64,2048]{1,0:T(8,128)(2,1)}) %reduce-scatter.5.cloned.1.call-update) | async-done | bytes 262160 | tf_op jit(solution)/shard_map/reduce_scatter | solution.py:155
  446.1 1.7 fusion.33
  (89 shorter events, 2.1 us)
Async XLA Ops:
  7.4 82.6 %copy-start = (bf16[256,2048]{1,0:T(8,128)(2,1)S(1)}, bf16[256,2048]{1,0:T(8,128)(2,1)}, u32[]{:S(2)}) copy-start(bf16[256,2048]{1,0:T(8,128)(2,1)} %param.29) | copy-start | bytes 3145732
  7.4 19.2 %copy-start.13 = (bf16[256,1,128]{2,0,1:T(8,128)(2,1)S(1)}, bf16[256,1,128]{2,0,1:T(8,128)(2,1)}, u32[]{:S(2)}) copy-start(bf16[256,1,128]{2,0,1:T(8,128)(2,1)} %param.25) | copy-start | bytes 196612
  7.4 110.1 %reduce-scatter.3.cloned.1.call-start = ((), (), s32[]{:S(2)}) async-start(), calls=%async_computation.2 | async-start | bytes 1310720 | tf_op jit(solution)/shard_map/reduce_scatter | solution.py:135
  41.9 8.3 %copy-start.14 = (bf16[256,1,128]{2,0,1:T(8,128)(2,1)S(1)}, bf16[256,1,128]{2,0,1:T(8,128)(2,1)}, u32[]{:S(2)}) copy-start(bf16[256,1,128]{2,0,1:T(8,128)(2,1)} %param.21) | copy-start | bytes 196612
  41.9 0.8 copy-start.1
  43.2 1.0 copy-start.8
  43.2 1.1 copy-start.11
  43.6 2.1 copy-start.2
  44.9 0.8 copy-start.9
  45.8 0.8 copy-start.1
  47.0 1.0 copy-start.8
  47.0 1.1 copy-start.11
  47.5 2.1 copy-start.2
  48.8 0.8 copy-start.9
  49.6 31.1 %copy-start.12 = (bf16[256,2,128]{2,1,0:T(2,128)(2,1)S(1)}, bf16[256,2,128]{2,1,0:T(2,128)(2,1)}, u32[]{:S(2)}) copy-start(bf16[256,2,128]{2,1,0:T(2,128)(2,1)} %param.20) | copy-start | bytes 393220
  81.3 1.0 copy-start.6
  81.4 1.1 copy-start.10
  83.1 0.8 copy-start.7
  84.4 1.0 copy-start.6
  84.4 1.1 copy-start.10
  86.2 0.8 copy-start.7
  87.0 2.6 copy-start.15
  87.0 2.6 copy-start.17
  87.0 2.6 copy-start.18
  87.0 2.8 copy-start.19
  89.8 1.2 copy-start.5
  92.4 0.7 copy-start.16
  92.4 25.1 %copy-start.3 = (bf16[64,2048]{1,0:T(8,128)(2,1)S(1)}, bf16[64,2048]{1,0:T(8,128)(2,1)}, u32[]{:S(2)}) copy-start(bf16[64,2048]{1,0:T(8,128)(2,1)} %param.19) | copy-start | bytes 786436
  92.5 151.6 %all-gather.9.cloned.1.call-start = ((), (), s32[]{:S(2)}) async-start(), calls=%async_computation.6 | async-start | bytes 10485760 | tf_op jit(solution)/shard_map/all_gather | solution.py:121
  93.0 167.3 %all-gather.5.cloned.1.call-start = ((), (), s32[]{:S(2)}) async-start(), calls=%async_computation.3 | async-start | bytes 1310720 | tf_op jit(solution)/shard_map/all_gather | solution.py:150
  120.5 290.8 %all-gather.7.cloned.1.call-start = ((), (), s32[]{:S(2)}) async-start(), calls=%async_computation.4 | async-start | bytes 10485760 | tf_op jit(solution)/shard_map/all_gather | solution.py:151
  121.0 325.1 %reduce-scatter.5.cloned.1.call-start = ((), (), s32[]{:S(2)}) async-start(), calls=%async_computation.5 | async-start | bytes 1310720 | tf_op jit(solution)/shard_map/reduce_scatter | solution.py:155
  411.3 34.8 %copy-start.4 = (bf16[64,2048]{1,0:T(8,128)(2,1)S(1)}, bf16[64,2048]{1,0:T(8,128)(2,1)}, u32[]{:S(2)}) copy-start(bf16[64,2048]{1,0:T(8,128)(2,1)} %reduce-scatter.3.cloned.1.call-done) | copy-start | bytes 786436
Sparse Core Ops, SparseCore 0:
  92.6 24.8 reduce-scatter.2
  423.1 22.9 reduce-scatter.4
Sparse Core Ops, SparseCore 1:
  94.5 149.5 all-gather.8
  245.5 14.7 all-gather.4
  261.8 149.4 all-gather.6
